TPU v7x, 32 devices: a whole 2x2x4 slice. The times are simulated.
32 devices in a mesh: fs: 8 (over z, x), tp: 4 (over y, core).
Axes of the slice: x: 2, y: 2, z: 4, core: 2. Of those that a mesh axis runs over, the one named last changes fastest.
Arguments:
- normed_input: bfloat16 [8192, 2048], P('fs'), may hold values from -64 to 64
- query_cotangent: bfloat16 [8192, 1024], P('fs', 'tp'), may hold values from -6 to 6
- key_cotangent: bfloat16 [8192, 512], P('fs', 'tp'), may hold values from -6 to 6
- query_weight: float32 [2048, 1024], P('fs', 'tp'), may hold values from -6 to 6
- key_weight: float32 [2048, 512], P('fs', 'tp'), may hold values from -6 to 6
- query_basis: bfloat16 [1024, 128], P('tp'), may hold values from -1 to 1
- key_basis: bfloat16 [512, 128], P('tp'), may hold values from -1 to 1
- moment_mean: float32 [2, 2048, 128], P(None, 'fs'), may hold values from -3 to 3
- moment_square: float32 [2, 2048, 128], P(None, 'fs'), may hold values from 0.25 to 4
Outputs:
- query_step: float32 [2048, 1024], P('fs', 'tp')
- key_step: float32 [2048, 512], P('fs', 'tp')
- query_updated: float32 [2048, 1024], P('fs', 'tp')
- key_updated: float32 [2048, 512], P('fs', 'tp')
- query_copy: bfloat16 [2048, 1024], P('fs', 'tp')
- key_copy: bfloat16 [2048, 512], P('fs', 'tp')
- mean_updated: float32 [2, 2048, 128], P(None, 'fs')
- square_updated: float32 [2, 2048, 128], P(None, 'fs')
All inputs are finite; a program needn't handle non-finite values.
Results may differ from a plain program's by a relative error of at most 0.0011.
Values sent between devices are 32-bit elements; how exact they have to be, the bound alone decides.
A program may use at most 64 MiB of HBM per device.

v0:
```python
import jax
import jax.numpy as jnp
from jax import lax
from jax.sharding import PartitionSpec as P

BETA_MEAN = 0.75
BETA_SQUARE = 0.8
STEP_RATE = 0.25
EPSILON = 1e-06


def local(
    normed_input,
    query_cotangent,
    key_cotangent,
    query_weight,
    key_weight,
    query_basis,
    key_basis,
    moment_mean,
    moment_square,
):
    highest = lax.Precision.HIGHEST
    contract = (((0,), (0,)), ((), ()))
    row_count = query_weight.shape[0]
    rank_width = query_basis.shape[1]
    query_float = query_basis.astype(jnp.float32)
    key_float = key_basis.astype(jnp.float32)
    partial_precision = lax.Precision.HIGH
    query_part = lax.dot_general(
        normed_input, query_cotangent, contract, preferred_element_type=jnp.float32
    )
    key_part = lax.dot_general(
        normed_input, key_cotangent, contract, preferred_element_type=jnp.float32
    )
    query_part, key_part = (query_part, key_part)
    summed = lax.psum_scatter(
        jnp.concatenate(
            [
                jnp.dot(query_part, query_float, precision=partial_precision),
                jnp.dot(key_part, key_float, precision=partial_precision),
            ],
            axis=1,
        ),
        "fs",
        scatter_dimension=0,
        tiled=True,
    )
    query_projected = summed[:, :rank_width]
    key_projected = summed[:, rank_width:]
    projected = lax.psum(jnp.stack([query_projected, key_projected]), "tp")
    total_square = lax.psum(jnp.sum(projected * projected), "fs")
    entry_count = 2.0 * row_count * lax.axis_size("fs") * rank_width
    normalized = projected * lax.rsqrt(total_square / entry_count + EPSILON)
    mean_updated = BETA_MEAN * moment_mean + (1.0 - BETA_MEAN) * normalized
    square_updated = BETA_SQUARE * moment_square + (1.0 - BETA_SQUARE) * normalized * normalized
    direction = mean_updated / jnp.sqrt(square_updated)
    outer = (((1,), (1,)), ((), ()))
    query_step = lax.dot_general(direction[0], query_float, outer, precision=highest)
    key_step = lax.dot_general(direction[1], key_float, outer, precision=highest)
    query_updated = query_weight - STEP_RATE * query_step
    key_updated = key_weight - STEP_RATE * key_step
    return (
        query_step,
        key_step,
        query_updated,
        key_updated,
        query_updated.astype(jnp.bfloat16),
        key_updated.astype(jnp.bfloat16),
        mean_updated,
        square_updated,
    )


def solution(mesh):
    in_specs = (
        P("fs", None),
        P("fs", "tp"),
        P("fs", "tp"),
        P("fs", "tp"),
        P("fs", "tp"),
        P("tp", None),
        P("tp", None),
        P(None, "fs", None),
        P(None, "fs", None),
    )
    out_specs = (
        P("fs", "tp"),
        P("fs", "tp"),
        P("fs", "tp"),
        P("fs", "tp"),
        P("fs", "tp"),
        P("fs", "tp"),
        P(None, "fs", None),
        P(None, "fs", None),
    )
    return jax.shard_map(local, mesh=mesh, in_specs=in_specs, out_specs=out_specs, check_vma=False)
```

profile of v0, /device:TPU:0, one launch (start us, length us, event | category | flops | bytes accessed | tf_op | source)
XLA Modules:
  0.0 158.6 jit_solution(541091675263221760)
XLA Ops:
  7.2 0.0 copy-start
  7.2 0.0 copy-start.2
  7.2 0.0 reduce-scatter.2.cloned.1.call-start
  7.2 1.0 copy-done
  8.2 0.0 copy-start.1
  8.2 3.7 %fusion.6 = f32[2048,256]{1,0:T(8,128)S(1)} fusion(bf16[1024,2048]{1,0:T(8,128)(2,1)} %param.9, bf16[1024,256]{1,0:T(8,128)(2,1)S(1)} %copy-done), kind=kOutput, calls=%fused_computation.17 | convolution fusion | flops 1073741824 | bytes 6815744 | tf_op jit(solution)/shard_map/dot_general | solution.py:30
  11.9 0.0 copy-done.2
  11.9 0.0 copy-done.1
  11.9 0.0 copy-start.4
  11.9 1.3 fusion.8
  13.2 0.0 copy-done.4
  13.3 0.0 copy-start.7
  13.3 0.8 fusion.7
  14.1 0.0 copy-done.7
  14.1 0.5 fusion.9
  14.6 1.5 pad_maximum_fusion
  16.1 0.0 copy-start.5
  16.1 0.0 copy-start.6
  16.1 0.0 reduce-scatter.2.cloned.1.call-update
  16.1 0.0 copy-start.3
  16.2 0.0 all-reduce.2.cloned.1.call-start
  16.2 72.0 %reduce-scatter.2.cloned.1.call-done = f32[256,256]{0,1:T(8,128)} async-done(((f32[2048,256]{0,1:T(8,128)}), f32[256,256]{0,1:T(8,128)}) %reduce-scatter.2.cloned.1.call-update) | async-done | bytes 262160 | tf_op jit(solution)/shard_map/reduce_scatter | solution.py:37
  88.2 1.0 slice_bitcast_fusion.5
  89.2 0.7 pad_maximum_fusion.1
  89.9 0.0 copy-start.8
  89.9 0.0 all-reduce.2.cloned.1.call-update
  89.9 0.0 copy-done.5
  89.9 0.1 copy.17
  90.0 32.4 %all-reduce.2.cloned.1.call-done = f32[2,256,128]{1,2,0:T(8,128)} async-done(((f32[2,256,128]{1,2,0:T(8,128)}), f32[2,256,128]{1,2,0:T(8,128)}) %all-reduce.2.cloned.1.call-update) | async-done | bytes 262160 | tf_op jit(solution)/shard_map/psum | solution.py:51
  122.4 1.6 %multiply_reduce_fusion = f32[]{:T(128)} fusion(f32[2,256,128]{1,2,0:T(8,128)} %all-reduce.2.cloned.1.call-done), kind=kLoop, calls=%fused_computation.7 | loop fusion | flops 131071 | bytes 262148 | tf_op jit(solution)/shard_map/reduce_sum | solution.py:52
  124.1 0.0 copy-done.6
  124.1 0.1 copy.18
  124.2 22.0 %psum.15 = f32[]{:T(128)} all-reduce(f32[]{:T(128)} %multiply_reduce_fusion), channel_id=1, replica_groups=mesh['fs'=8,'tp'=4] {'fs'}, use_global_device_ids=true, to_apply=%region_3.0 | all-reduce | flops 1 | bytes 8 | tf_op jit(solution)/shard_map/psum | solution.py:52
  146.9 1.0 rsqrt_multiply_fusion
  147.9 0.0 copy-done.3
  147.9 1.1 fusion.4
  149.1 0.0 copy-done.8
  149.1 1.0 fusion.3
  150.1 0.8 copy.19
  150.9 0.8 copy.20
Async XLA Ops:
  7.2 1.0 copy-start
  7.2 4.7 %copy-start.2 = (bf16[1024,128]{1,0:T(8,128)(2,1)S(1)}, bf16[1024,128]{1,0:T(8,128)(2,1)}, u32[]{:S(2)}) copy-start(bf16[1024,128]{1,0:T(8,128)(2,1)} %param.11) | copy-start | bytes 786436
  7.2 81.0 %reduce-scatter.2.cloned.1.call-start = ((), (), s32[]{:S(2)}) async-start(), calls=%async_computation.1 | async-start | bytes 2359296 | tf_op jit(solution)/shard_map/reduce_scatter | solution.py:37
  8.2 3.7 %copy-start.1 = (bf16[1024,2048]{1,0:T(8,128)(2,1)S(1)}, bf16[1024,2048]{1,0:T(8,128)(2,1)}, u32[]{:S(2)}) copy-start(bf16[1024,2048]{1,0:T(8,128)(2,1)} %param.9) | copy-start | bytes 12582916
  11.9 1.3 copy-start.4
  13.3 0.9 copy-start.7
  16.1 73.8 %copy-start.5 = (f32[2,256,128]{2,1,0:T(8,128)S(1)}, f32[2,256,128]{2,1,0:T(8,128)}, u32[]{:S(2)}) copy-start(f32[2,256,128]{2,1,0:T(8,128)} %param.16) | copy-start | bytes 786436
  16.1 107.9 %copy-start.6 = (f32[2,256,128]{2,1,0:T(8,128)S(1)}, f32[2,256,128]{2,1,0:T(8,128)}, u32[]{:S(2)}) copy-start(f32[2,256,128]{2,1,0:T(8,128)} %param.17) | copy-start | bytes 786436
  16.1 131.8 %copy-start.3 = (f32[256,256]{1,0:T(8,128)S(1)}, f32[256,256]{1,0:T(8,128)}, u32[]{:S(2)}) copy-start(f32[256,256]{1,0:T(8,128)} %param.12) | copy-start | bytes 786436
  16.2 106.3 %all-reduce.2.cloned.1.call-start = ((), (), s32[]{:S(2)}) async-start(), calls=%async_computation.2 | async-start | bytes 524288 | tf_op jit(solution)/shard_map/psum | solution.py:51
  89.9 59.2 %copy-start.8 = (f32[256,128]{1,0:T(8,128)S(1)}, f32[256,128]{1,0:T(8,128)}, u32[]{:S(2)}) copy-start(f32[256,128]{1,0:T(8,128)} %param.13) | copy-start | bytes 393220
Sparse Core Ops, SparseCore 0:
  16.3 71.8 reduce-scatter.1
  91.1 31.3 all-reduce.1
where the time goes:
time: 159 us
  waiting for transfers between devices  104 us (65%)
  blocking collectives  22 us (14%)
  between operations  14.9 us (9%)
  matrix products  8.46 us (5%)
  other arithmetic  4.88 us (3%)
  local copies, waits for them, and re-layouts  3.93 us (2%)
    reduce_scatter x1, waiting for transfers between devices, local(): lax.psum_scatter(jnp.concatenate([jnp.dot(query_part, query_float, precis...  72 us
    psum x1, waiting for transfers between devices, local(): projected = lax.psum(jnp.stack([query_projected, key_projected]), 'tp')  32.4 us
    psum x1, blocking collectives, local(): total_square = lax.psum(jnp.sum(projected * projected), 'fs')  22 us
    dot_general x1, matrix products, local(): lax.dot_general(normed_input, query_cotangent, contract, preferred_elemen...  3.68 us
  transfers between devices with their start and end apart: 2, of which 2 were waited for; matrix products, arithmetic and copies ran while one was open for 0% of the time, Pallas kernels for 0%

commit v1 on v0

--- a/solution.py
+++ b/solution.py
@@ -2,6 +2,7 @@
 import jax.numpy as jnp
 from jax import lax
 from jax.sharding import PartitionSpec as P
+from jax.lax import all_gather
 
 BETA_MEAN = 0.75
 BETA_SQUARE = 0.8
@@ -48,7 +49,9 @@
     )
     query_projected = summed[:, :rank_width]
     key_projected = summed[:, rank_width:]
-    projected = lax.psum(jnp.stack([query_projected, key_projected]), "tp")
+    field = jnp.stack([query_projected, key_projected])
+    x_now = all_gather(field, "tp")
+    projected = jnp.sum(x_now, axis=0)
     total_square = lax.psum(jnp.sum(projected * projected), "fs")
     entry_count = 2.0 * row_count * lax.axis_size("fs") * rank_width
     normalized = projected * lax.rsqrt(total_square / entry_count + EPSILON)

time: 159 us -> 142 us (0.89)
  waiting for transfers between devices: 104 us -> 87.8 us
    psum x1 -> x0, waiting for transfers between devices: 32.4 us -> none  [local(): projected = lax.psum(jnp.stack([query_projected, key_projected]), 'tp')]
    all_gather x0 -> x1, waiting for transfers between devices: none -> 15.9 us  [local(): x_now = all_gather(field, 'tp')]
where the time goes in v1:
time: 142 us
  waiting for transfers between devices  87.8 us (62%)
  blocking collectives  22 us (15%)
  between operations  14.9 us (10%)
  matrix products  8.46 us (6%)
  local copies, waits for them, and re-layouts  4.9 us (3%)
  other arithmetic  3.62 us (3%)
    reduce_scatter x1, waiting for transfers between devices, local(): lax.psum_scatter(jnp.concatenate([jnp.dot(query_part, query_float, precis...  71.9 us
    psum x1, blocking collectives, local(): total_square = lax.psum(jnp.sum(projected * projected), 'fs')  22 us
    all_gather x1, waiting for transfers between devices, local(): x_now = all_gather(field, 'tp')  15.9 us
    dot_general x1, matrix products, local(): lax.dot_general(normed_input, query_cotangent, contract, preferred_elemen...  3.68 us
    unnamed x23, local copies, waits for them, and re-layouts  3.08 us
  transfers between devices with their start and end apart: 2, of which 2 were waited for; matrix products, arithmetic and copies ran while one was open for 0% of the time, Pallas kernels for 0%

profile of v1, /device:TPU:0, one launch (start us, length us, event | category | flops | bytes accessed | tf_op | source)
XLA Modules:
  0.0 141.8 jit_solution(13027463954613374363)
XLA Ops:
  7.2 0.0 copy-start
  7.2 0.0 copy-start.2
  7.2 0.0 reduce-scatter.2.cloned.1.call-start
  7.2 1.0 copy-done
  8.2 0.0 copy-start.1
  8.2 3.7 %fusion.6 = f32[2048,256]{1,0:T(8,128)S(1)} fusion(bf16[1024,2048]{1,0:T(8,128)(2,1)} %param.9, bf16[1024,256]{1,0:T(8,128)(2,1)S(1)} %copy-done), kind=kOutput, calls=%fused_computation.17 | convolution fusion | flops 1073741824 | bytes 6815744 | tf_op jit(solution)/shard_map/dot_general | solution.py:31
  11.9 0.0 copy-done.2
  11.9 0.0 copy-done.1
  11.9 0.0 copy-start.4
  11.9 1.3 fusion.8
  13.2 0.0 copy-done.4
  13.3 0.0 copy-start.7
  13.3 0.8 fusion.7
  14.1 0.0 copy-done.7
  14.1 0.5 fusion.9
  14.6 1.5 %pad_maximum_fusion = f32[2048,256]{0,1:T(8,128)} fusion(f32[2048,128]{0,1:T(8,128)S(1)} %fusion.9, f32[2048,128]{0,1:T(8,128)S(1)} %fusion.7), kind=kLoop, calls=%fused_computation | loop fusion | flops 524288 | bytes 4194304 | tf_op jit(solution)/shard_map/concatenate | solution.py:39
  16.1 0.0 copy-start.5
  16.1 0.0 reduce-scatter.2.cloned.1.call-update
  16.1 0.0 all-gather.3.cloned.1.call-start
  16.2 71.9 %reduce-scatter.2.cloned.1.call-done = f32[256,256]{0,1:T(8,128)} async-done(((f32[2048,256]{0,1:T(8,128)}), f32[256,256]{0,1:T(8,128)}) %reduce-scatter.2.cloned.1.call-update) | async-done | bytes 262160 | tf_op jit(solution)/shard_map/reduce_scatter | solution.py:38
  88.1 1.0 slice_bitcast_fusion.5
  89.1 0.0 copy-start.6
  89.1 0.8 copy.18
  89.9 0.0 all-gather.3.cloned.1.call-update
  90.0 0.0 copy-done.5
  90.0 0.1 copy.17
  90.1 15.9 %all-gather.3.cloned.1.call-done = f32[8,256,128]{2,1,0:T(8,128)} async-done(((f32[2,256,128]{2,1,0:T(8,128)}), f32[8,256,128]{2,1,0:T(8,128)}) %all-gather.3.cloned.1.call-update) | async-done | bytes 1048592 | tf_op jit(solution)/shard_map/all_gather | solution.py:53
  106.0 0.0 copy-start.3
  106.0 1.3 reduce_sum.18
  107.4 0.0 copy-start.8
  107.4 0.1 copy.23
  107.5 0.7 multiply_reduce_fusion
  108.2 0.0 copy-done.6
  108.2 0.1 copy.20
  108.3 22.0 %psum.7 = f32[]{:T(128)} all-reduce(f32[]{:T(128)} %multiply_reduce_fusion), channel_id=1, replica_groups=mesh['fs'=8,'tp'=4] {'fs'}, use_global_device_ids=true, to_apply=%region_3.0 | all-reduce | flops 1 | bytes 8 | tf_op jit(solution)/shard_map/psum | solution.py:55
  131.0 0.1 rsqrt_multiply_fusion
  131.1 0.0 copy-done.3
  131.1 1.1 fusion.4
  132.2 0.0 copy-done.8
  132.2 1.0 fusion.3
  133.3 0.8 copy.21
  134.1 0.8 copy.22
  (1 shorter events, 0.0 us)
Async XLA Ops:
  7.2 1.0 copy-start
  7.2 4.7 %copy-start.2 = (bf16[1024,128]{1,0:T(8,128)(2,1)S(1)}, bf16[1024,128]{1,0:T(8,128)(2,1)}, u32[]{:S(2)}) copy-start(bf16[1024,128]{1,0:T(8,128)(2,1)} %param.11) | copy-start | bytes 786436
  7.2 80.9 %reduce-scatter.2.cloned.1.call-start = ((), (), s32[]{:S(2)}) async-start(), calls=%async_computation.1 | async-start | bytes 2359296 | tf_op jit(solution)/shard_map/reduce_scatter | solution.py:38
  8.2 3.7 %copy-start.1 = (bf16[1024,2048]{1,0:T(8,128)(2,1)S(1)}, bf16[1024,2048]{1,0:T(8,128)(2,1)}, u32[]{:S(2)}) copy-start(bf16[1024,2048]{1,0:T(8,128)(2,1)} %param.9) | copy-start | bytes 12582916
  11.9 1.3 copy-start.4
  13.3 0.9 copy-start.7
  16.1 73.9 %copy-start.5 = (f32[2,256,128]{2,1,0:T(8,128)S(1)}, f32[2,256,128]{2,1,0:T(8,128)}, u32[]{:S(2)}) copy-start(f32[2,256,128]{2,1,0:T(8,128)} %param.16) | copy-start | bytes 786436
  16.1 89.9 %all-gather.3.cloned.1.call-start = ((), (), s32[]{:S(2)}) async-start(), calls=%async_computation.2 | async-start | bytes 1310720 | tf_op jit(solution)/shard_map/all_gather | solution.py:53
  89.1 19.1 %copy-start.6 = (f32[2,256,128]{2,1,0:T(8,128)S(1)}, f32[2,256,128]{2,1,0:T(8,128)}, u32[]{:S(2)}) copy-start(f32[2,256,128]{2,1,0:T(8,128)} %param.17) | copy-start | bytes 786436
  106.0 25.1 %copy-start.3 = (f32[256,256]{1,0:T(8,128)S(1)}, f32[256,256]{1,0:T(8,128)}, u32[]{:S(2)}) copy-start(f32[256,256]{1,0:T(8,128)} %param.12) | copy-start | bytes 786436
  107.4 24.9 %copy-start.8 = (f32[256,128]{1,0:T(8,128)S(1)}, f32[256,128]{1,0:T(8,128)}, u32[]{:S(2)}) copy-start(f32[256,128]{1,0:T(8,128)} %param.13) | copy-start | bytes 393220
Sparse Core Ops, SparseCore 0:
  16.3 71.7 reduce-scatter.1
  90.2 15.7 all-gather.2
